TPU v7x, 256 devices: a 4x2x16 block of a 4x16x16 slice. The times are simulated.
256 devices in a mesh: grp: 2 (over y), sp: 16 (over z), tp: 4 (over x), dp: 2 (over core).
Axes of the slice: x: 4, y: 2, z: 16, core: 2. Of those that a mesh axis runs over, the one named last changes fastest.
The devices are a block of a 4x16x16 slice.
Arguments:
- latent: bfloat16 [24576, 4096], P(('grp', 'sp', 'dp')), parts along dimension 0, may hold values from -6 to 6
- context: bfloat16 [1024, 4096], P(('grp', 'sp')), parts along dimension 0, may hold values from -6 to 6
- condition: bfloat16 [8192], P('grp'), parts along dimension 0, may hold values from -6 to 6
- context_condition: bfloat16 [4096], replicated, may hold values from -6 to 6
- shift_weight: bfloat16 [4096, 4096], P('sp', ('tp', 'dp')), may hold values from -0.09375 to 0.09375
- scale_weight: bfloat16 [4096, 4096], P('sp', ('tp', 'dp')), may hold values from -0.09375 to 0.09375
- gate_weight: bfloat16 [4096, 4096], P('sp', ('tp', 'dp')), may hold values from -0.09375 to 0.09375
- norm_gain: float32 [4096], replicated, may hold values from 0.1 to 1.9
- out_gate_weight: bfloat16 [4096, 2048], P(None, ('tp', 'dp')), may hold values from -0.09375 to 0.09375
- signal_weight: bfloat16 [4096, 2048], P(None, ('tp', 'dp')), may hold values from -0.09375 to 0.09375
- writer_weight: bfloat16 [4096, 1024], P(None, ('tp', 'dp')), may hold values from -0.09375 to 0.09375
- reader_matrix: bfloat16 [4096, 1024], P(None, ('tp', 'dp')), may hold values from -0.09375 to 0.09375
- step_weight: bfloat16 [2, 4096, 32], P(None, None, ('tp', 'dp')), may hold values from -0.09375 to 0.09375
- signal_taps: float32 [3, 2048], P(None, ('tp', 'dp')), may hold values from -3.5 to 3.5
- writer_taps: float32 [3, 1024], P(None, ('tp', 'dp')), may hold values from -3.5 to 3.5
- reader_taps: float32 [3, 1024], P(None, ('tp', 'dp')), may hold values from -3.5 to 3.5
- step_bias: float32 [2, 32], P(None, ('tp', 'dp')), may hold values from -4.5 to -2.5
- decay_log: float32 [2, 32], P(None, ('tp', 'dp')), may hold values from -12 to 1
- decay_extra: float32 [2, 32, 24576], P(None, ('tp', 'dp'), ('grp', 'sp')), parts along dimension 2, may hold values from -3 to 0
- group_gain: float32 [2048], P(('tp', 'dp')), may hold values from 0.1 to 1.9
- output_weight: bfloat16 [2048, 4096], P(None, ('tp', 'dp')), may hold values from -0.125 to 0.125
Outputs:
- updated: bfloat16 [24576, 4096], P(('grp', 'sp'), ('tp', 'dp')), parts along dimension 0
There are 2 independent parts, one for each index of `grp`. A program takes and returns all parts, laid end to end along the dimension named above; an argument that names none is the same for every part. Nothing has to cross between parts.
All inputs are finite; a program needn't handle non-finite values.
Results may differ from a plain program's by a relative error of at most 0.007.
Values may be sent and summed in bfloat16 or wider, within the bound.
No kernel may reach another device: no remote copies, remote signals or barrier semaphores. Data moves between devices by JAX's collectives and lax.ppermute only.
A program may use at most 128 MiB of HBM per device.

v0:
```python
import jax
import jax.numpy as jnp
from jax import lax
from jax.sharding import PartitionSpec as P

STATE = 128
BLOCK = 128
EPSILON = 1e-06


def copy_for_each(x, axis):
    copies = jnp.broadcast_to(x, (lax.axis_size(axis), *x.shape))
    return lax.all_to_all(copies, axis, split_axis=0, concat_axis=0, tiled=True)


def of_everyone(x, axis):
    everything = copy_for_each(x, axis)
    return jnp.sum(everything, axis=0)


def in_one(arrays, axis):
    ends = [0]
    for a in arrays:
        ends.append(ends[-1] + a.size)
    subtotal = of_everyone(jnp.concatenate([a.ravel() for a in arrays]), axis)
    return tuple((subtotal[b:e].reshape(a.shape) for a, b, e in zip(arrays, ends, ends[1:])))


def side_by_side(arrays, axis, dim, along):
    ends, at = ([], 0)
    for a in arrays[:-1]:
        at += a.shape[along]
        ends.append(at)
    both = jnp.concatenate(arrays, axis=along)
    return tuple(jnp.split(lax.all_gather(both, axis, axis=dim, tiled=True), ends, axis=along))


def rows_first(arrays, axis, dims):
    turned = [jnp.moveaxis(a, dim, 0) for a, dim in zip(arrays, dims)]
    widths = [t[0].size for t in turned]
    both = jnp.concatenate([t.reshape(-1, w) for t, w in zip(turned, widths)], axis=1)
    out = lax.all_gather(both, axis, axis=0, tiled=True)
    tiles = jnp.split(out, [sum(widths[:k]) for k in range(1, len(widths))], axis=1)
    return tuple(
        (
            jnp.moveaxis(b.reshape(-1, *t.shape[1:]), 0, dim)
            for b, t, dim in zip(tiles, turned, dims)
        )
    )


def extended(cells, sides, width):
    for axis, dim in sides:
        count = lax.axis_size(axis)
        ends = count - 1
        head = lax.slice_in_dim(cells, 0, width, axis=dim)
        tail = lax.slice_in_dim(cells, cells.shape[dim] - width, cells.shape[dim], axis=dim)
        cells = jnp.concatenate(
            [
                lax.ppermute(tail, axis, [(i, (i + 1) % count) for i in range(ends)]),
                cells,
                lax.ppermute(head, axis, [((i + 1) % count, i) for i in range(ends)]),
            ],
            axis=dim,
        )
    return cells


def entering(x, axis, combine, identity, reverse):
    devices, position = (lax.axis_size(axis), lax.axis_index(axis))
    everything = jax.tree.map(lambda part: lax.all_gather(part, axis), x)
    start = jax.tree.map(
        lambda part, zero: jnp.broadcast_to(jnp.asarray(zero, part.dtype), part.shape), x, identity
    )

    def turn(k, before):
        at = devices - 1 - k if reverse else k
        reached = at > position if reverse else at < position
        new = combine(before, jax.tree.map(lambda part: part[at], everything))
        return jax.tree.map(lambda a, b: jnp.where(reached, a, b), new, before)

    return lax.fori_loop(0, devices, turn, start)


def modulate(rows, norm_gain, shift_vec, scale_vec):
    values = rows.astype(jnp.float32)
    normed = (
        values * lax.rsqrt(jnp.mean(values * values, axis=-1, keepdims=True) + EPSILON) * norm_gain
    )
    return (normed * (1.0 + scale_vec) + shift_vec).astype(jnp.bfloat16)


def centred_conv(padded, conv_taps, length):
    running = jnp.zeros((length, padded.shape[1]), jnp.float32)
    for offset in range(conv_taps.shape[0]):
        running = running + conv_taps[offset] * padded[offset : offset + length].astype(jnp.float32)
    return jax.nn.silu(running)


def project_rows(hidden, signal_weight, writer_weight, reader_matrix, step_weight):
    raw_cols = jnp.concatenate(
        [
            jnp.dot(hidden, signal_weight, preferred_element_type=jnp.float32),
            jnp.dot(hidden, writer_weight, preferred_element_type=jnp.float32),
            jnp.dot(hidden, reader_matrix, preferred_element_type=jnp.float32),
        ],
        axis=1,
    ).astype(jnp.bfloat16)
    step_in = jnp.stack(
        [
            jnp.dot(hidden, step_weight[0], preferred_element_type=jnp.float32),
            jnp.dot(hidden, step_weight[1], preferred_element_type=jnp.float32),
        ]
    ).astype(jnp.bfloat16)
    return (raw_cols, step_in)


def split_mixed(conv_out, head_count, head_width, group_count, state_width):
    length = conv_out.shape[0]
    signal_end = head_count * head_width
    writer_end = signal_end + group_count * state_width
    signal = conv_out[:, :signal_end].reshape(length, head_count, head_width)
    writer = conv_out[:, signal_end:writer_end].reshape(length, group_count, state_width)
    reader = conv_out[:, writer_end:].reshape(length, group_count, state_width)
    return (signal, writer, reader)


def state_span(signal, step_size, log_decay, writer, reader, start_state, block):
    length, head_count, head_width = signal.shape
    group_count, state_width = (writer.shape[1], writer.shape[2])
    per_group = head_count // group_count
    blocks = length // block
    scaled = (signal * step_size[..., None]).reshape(
        blocks, block, group_count, per_group, head_width
    )
    cum_log = jnp.cumsum(log_decay.reshape(blocks, block, group_count, per_group), axis=1)
    writer_blk = writer.reshape(blocks, block, group_count, state_width)
    reader_blk = reader.reshape(blocks, block, group_count, state_width)
    inner_dot = jnp.einsum("bign,bjgn->bgij", reader_blk, writer_blk)
    moved = jnp.moveaxis(cum_log, 1, -1)
    gap_logs = moved[..., :, None] - moved[..., None, :]
    lower_mask = jnp.tril(jnp.ones((block, block), dtype=bool))
    weights = jnp.exp(jnp.where(lower_mask, gap_logs, -jnp.inf))
    in_block = jnp.einsum("bgij,bgeij,bjgep->bigep", inner_dot, weights, scaled)
    to_end = jnp.exp(cum_log[:, -1:] - cum_log)
    states = jnp.einsum("bjgn,bjge,bjgep->bgepn", writer_blk, to_end, scaled)
    block_decay = jnp.exp(cum_log[:, -1])

    def advance(running, block_item):
        state_add, decay_now = block_item
        return (running * decay_now[..., None, None] + state_add, running)

    last_state, before = lax.scan(
        advance,
        start_state.reshape(group_count, per_group, head_width, state_width),
        (states, block_decay),
    )
    carried = jnp.einsum("bign,bgepn,bige->bigep", reader_blk, before, jnp.exp(cum_log))
    result = (in_block + carried).reshape(length, head_count, head_width)
    return (result, last_state.reshape(head_count, head_width, state_width))


def context_state(signal, row_weights, writer):
    length, head_count, head_width = signal.shape
    group_count, state_width = (writer.shape[1], writer.shape[2])
    per_group = head_count // group_count
    grouped = signal.reshape(length, group_count, per_group, head_width)
    weights = row_weights.reshape(length, group_count, per_group)
    summed = jnp.einsum("tgn,tge,tgep->gepn", writer, weights, grouped)
    return summed.reshape(head_count, head_width, state_width)


def group_norm(gated, group_count, group_gain):
    length = gated.shape[0]
    grouped = gated.reshape(length, group_count, -1)
    normed = grouped * lax.rsqrt(jnp.mean(grouped * grouped, axis=-1, keepdims=True) + EPSILON)
    return (normed.reshape(length, -1) * group_gain).astype(jnp.bfloat16)


def chain_step(preceding_entries, later):
    return (
        preceding_entries[0] + later[0],
        jnp.exp(later[0])[:, None, None] * preceding_entries[1] + later[1],
    )


def on_device(
    latent,
    context,
    condition,
    context_condition,
    shift_weight,
    scale_weight,
    gate_weight,
    norm_gain,
    out_gate_weight,
    signal_weight,
    writer_weight,
    reader_matrix,
    step_weight,
    signal_taps,
    writer_taps,
    reader_taps,
    step_bias,
    decay_log,
    decay_extra,
    group_gain,
    output_weight,
):
    rows_here = shift_weight.shape[0]
    cond_act = jax.nn.silu(jnp.stack([condition, context_condition]).astype(jnp.float32)).astype(
        jnp.bfloat16
    )
    own_rows = lax.dynamic_slice_in_dim(cond_act, lax.axis_index("sp") * rows_here, rows_here, 1)
    shift_part = jnp.dot(own_rows, shift_weight, preferred_element_type=jnp.float32)
    scale_part = jnp.dot(own_rows, scale_weight, preferred_element_type=jnp.float32)
    gate_part = jnp.dot(own_rows[:1], gate_weight, preferred_element_type=jnp.float32)
    shift_sum, scale_sum, gate_sum = in_one((shift_part, scale_part, gate_part), "sp")
    shift_vec, scale_vec = side_by_side((shift_sum, scale_sum), ("tp", "dp"), 1, 0)
    gate_vec = gate_sum[0]
    full_rows = lax.all_gather(latent, "dp", axis=0, tiled=True)
    length = full_rows.shape[0]
    hidden = modulate(full_rows, norm_gain, shift_vec[0], scale_vec[0])
    ctx_hidden = modulate(context, norm_gain, shift_vec[1], scale_vec[1])
    conv_taps = jnp.concatenate([signal_taps, writer_taps, reader_taps], axis=1)
    decay_rates = -jnp.exp(decay_log)[:, None, :]
    head_count = step_bias.shape[1]
    head_width = signal_weight.shape[1] // head_count
    group_count = writer_weight.shape[1] // STATE
    per_group = head_count // group_count
    ctx_raw, ctx_step_in = project_rows(
        ctx_hidden, signal_weight, writer_weight, reader_matrix, step_weight
    )
    every_raw, every_step = rows_first((ctx_raw, ctx_step_in), "sp", (0, 1))
    ctx_len = every_raw.shape[0]
    ctx_conv = centred_conv(jnp.pad(every_raw, ((1, 1), (0, 0))), conv_taps, ctx_len)
    ctx_signal, ctx_writer, _ = split_mixed(ctx_conv, head_count, head_width, group_count, STATE)
    prefix_stride_length = jax.nn.softplus(every_step.astype(jnp.float32) + step_bias[:, None, :])
    ctx_decay = decay_rates * prefix_stride_length
    cum_log = jnp.cumsum(ctx_decay, axis=1)
    ctx_forward = context_state(
        ctx_signal, jnp.exp(cum_log[0, -1:] - cum_log[0]) * prefix_stride_length[0], ctx_writer
    )
    ctx_backward = context_state(
        ctx_signal, jnp.exp(cum_log[1] - ctx_decay[1]) * prefix_stride_length[1], ctx_writer
    )
    gate_in = jnp.dot(hidden, out_gate_weight, preferred_element_type=jnp.float32).astype(
        jnp.bfloat16
    )
    raw_cols, step_in = project_rows(
        hidden, signal_weight, writer_weight, reader_matrix, step_weight
    )
    padded = extended(raw_cols, (("sp", 0),), 1)
    signal, writer, reader = split_mixed(
        centred_conv(padded, conv_taps, length), head_count, head_width, group_count, STATE
    )
    step_size = jax.nn.softplus(step_in.astype(jnp.float32) + step_bias[:, None, :])
    log_decay = decay_rates * step_size + jnp.swapaxes(decay_extra, 1, 2)
    zero_state = jnp.zeros((head_count, head_width, STATE), jnp.float32)
    forward_out, forward_last = state_span(
        signal, step_size[0], log_decay[0], writer, reader, zero_state, BLOCK
    )
    back_signal = jnp.flip(signal, 0)
    back_reader = jnp.flip(reader, 0)
    back_decay = jnp.flip(log_decay[1], 0)
    backward_out, backward_last = state_span(
        back_signal,
        jnp.flip(step_size[1], 0),
        back_decay,
        jnp.flip(writer, 0),
        back_reader,
        zero_state,
        BLOCK,
    )
    cum_forward = jnp.cumsum(log_decay[0], axis=0)
    cumulative_backward = jnp.cumsum(back_decay, axis=0)
    identity = (jnp.zeros((head_count,), jnp.float32), zero_state)
    onward_inflow = entering((cum_forward[-1], forward_last), "sp", chain_step, identity, False)
    enter_bwd = entering((cumulative_backward[-1], backward_last), "sp", chain_step, identity, True)
    start_fwd = jnp.exp(onward_inflow[0])[:, None, None] * ctx_forward + onward_inflow[1]
    start_bwd = jnp.exp(enter_bwd[0])[:, None, None] * ctx_backward + enter_bwd[1]
    reader_head_rows = jnp.repeat(reader, per_group, axis=1)
    back_heads = jnp.repeat(back_reader, per_group, axis=1)
    forward_out = (
        forward_out
        + jnp.einsum("thn,hpn->thp", reader_head_rows, start_fwd) * jnp.exp(cum_forward)[..., None]
    )
    backward_out = (
        backward_out
        + jnp.einsum("thn,hpn->thp", back_heads, start_bwd)
        * jnp.exp(cumulative_backward)[..., None]
    )
    both = (forward_out + jnp.flip(backward_out, 0)).reshape(length, -1)
    gated = both * jax.nn.silu(gate_in.astype(jnp.float32))
    normed = group_norm(gated, group_count, group_gain)
    mix = jnp.dot(
        lax.all_gather(normed, ("tp", "dp"), axis=1, tiled=True),
        output_weight,
        preferred_element_type=jnp.float32,
    )
    out_start = lax.axis_index(("tp", "dp")) * output_weight.shape[1]
    residual = lax.dynamic_slice_in_dim(full_rows, out_start, output_weight.shape[1], 1).astype(
        jnp.float32
    )
    return (residual + gate_vec * mix).astype(jnp.bfloat16)


def solution(mesh):
    in_specs = (
        P(("grp", "sp", "dp"), None),
        P(("grp", "sp"), None),
        P("grp"),
        P(),
        P("sp", ("tp", "dp")),
        P("sp", ("tp", "dp")),
        P("sp", ("tp", "dp")),
        P(),
        P(None, ("tp", "dp")),
        P(None, ("tp", "dp")),
        P(None, ("tp", "dp")),
        P(None, ("tp", "dp")),
        P(None, None, ("tp", "dp")),
        P(None, ("tp", "dp")),
        P(None, ("tp", "dp")),
        P(None, ("tp", "dp")),
        P(None, ("tp", "dp")),
        P(None, ("tp", "dp")),
        P(None, ("tp", "dp"), ("grp", "sp")),
        P(("tp", "dp")),
        P(None, ("tp", "dp")),
    )
    out_specs = P(("grp", "sp"), ("tp", "dp"))
    return jax.shard_map(
        on_device, mesh=mesh, in_specs=in_specs, out_specs=out_specs, check_vma=False
    )
```

profile of v0, /device:TPU:33, one launch (start us, length us, event | category | flops | bytes accessed | tf_op | source)
XLA Modules:
  0.0 478.3 jit_solution(13487710746028656442)
XLA Ops:
  8.9 24.5 %all-to-all-start = ((f32[16,1,2560]{2,1,0:T(1,128)}), f32[16,1,2560]{2,1,0:T(1,128)S(1)}, u32[]{:S(2)}, u32[]{:S(2)}) async-start(f32[16,1,2560]{2,1,0:T(1,128)} %broadcast_in_dim.34), calls=%async_computation | async-start | bytes 327680 | tf_op jit(solution)/shard_map/all_to_all | solution.py:13
  34.5 10.9 %all-to-all-done = f32[16,1,2560]{2,1,0:T(1,128)S(1)} async-done(((f32[16,1,2560]{2,1,0:T(1,128)}), f32[16,1,2560]{2,1,0:T(1,128)S(1)}, u32[]{:S(2)}, u32[]{:S(2)}) %all-to-all-start) | async-done | bytes 163872 | tf_op jit(solution)/shard_map/all_to_all | solution.py:13
  45.6 17.6 %all_gather.25 = f32[4,4096]{1,0:T(4,128)S(1)} all-gather(f32[4,512]{1,0:T(4,128)S(1)} %pad_maximum_fusion.9), channel_id=1, replica_groups=mesh['grp'=2,'sp'=16,'tp'=4,'dp'=2] {'tp','dp'}, dimensions={1}, use_global_device_ids=true | all-gather | bytes 73728 | tf_op jit(solution)/shard_map/all_gather | solution.py:35
  63.9 1.7 convolution_convert_fusion.5
  65.6 1.5 convolution_convert_fusion.6
  67.6 25.9 %all_gather.28 = bf16[512,520]{1,0:T(8,128)(2,1)S(1)} all-gather(bf16[32,520]{1,0:T(8,128)(2,1)S(1)} %pad_maximum_fusion.7), channel_id=1, replica_groups=mesh['grp'=2,'sp'=16,'tp'=4,'dp'=2] {'sp'}, dimensions={0}, use_global_device_ids=true | all-gather | bytes 565760 | tf_op jit(solution)/shard_map/all_gather | solution.py:42
  96.4 2.4 reduce-window.24
  101.1 4.2 fusion.4
  105.7 3.1 fusion.8
  108.9 2.2 convolution_convert_fusion.2
  111.1 2.2 convolution_convert_fusion.3
  113.4 2.0 convolution_convert_fusion.1
  115.4 1.7 fusion.38
  117.1 2.0 fusion.37
  121.2 4.7 collective-permute-start
  128.5 3.3 rev.19
  136.2 1.7 copy.341
  141.8 2.2 reduce-window.20
  148.3 1.7 fusion.107
  150.0 1.7 fusion.106
  151.7 1.8 copy.329
  153.5 1.7 copy.326
  159.8 1.7 copy.306
  161.5 20.6 %all-gather.1 = f32[16,1,4]{2,1,0:T(1,128)} all-gather(f32[1,1,4]{2,1,0:T(1,128)} %bitcast.351), channel_id=1, replica_groups=mesh['grp'=2,'sp'=16,'tp'=4,'dp'=2] {'sp'}, dimensions={0}, use_global_device_ids=true | all-gather | bytes 272 | tf_op jit(solution)/shard_map/all_gather | solution.py:71
  182.1 21.8 %all-gather = f32[16,1,4]{2,1,0:T(1,128)} all-gather(f32[1,1,4]{2,1,0:T(1,128)} %bitcast.352), channel_id=1, replica_groups=mesh['grp'=2,'sp'=16,'tp'=4,'dp'=2] {'sp'}, dimensions={0}, use_global_device_ids=true | all-gather | bytes 272 | tf_op jit(solution)/shard_map/all_gather | solution.py:71
  204.0 4.9 %divide_multiply_fusion = f32[768,512]{0,1:T(8,128)S(1)} fusion(bf16[1,512]{0,1:T(8,128)(2,1)S(1)} %collective-permute-done.1, bf16[768,128]{0,1:T(8,128)(2,1)S(1)} %copy-done.15, bf16[768,128]{0,1:T(8,128)(2,1)S(1)} %copy-done.17, bf16[768,256]{0,1:T(8,128)(2,1)} %copy-done.23, bf16[1,512]{0,1:T(8,128)(2,1)} %collective-permute-done, f32[512]{0:T(512)} %bitcast.339, ...), kind=kLoop, calls=%fused_computation.35 | loop fusion | flops 12189696 | bytes 2367488 | tf_op jit(solution)/shard_map/jit(silu)/mul | solution.py:97
  209.8 3.8 reverse.6
  213.5 1.8 copy.303
  215.3 3.8 reverse.7
  219.0 1.7 copy.304
  220.8 1.8 copy.323
  222.5 1.7 copy.324
  225.3 2.4 rev.18
  232.5 8.2 %while.62 = (s32[]{:T(128)}, f32[1,4,64,128]{3,2,1,0:T(8,128)S(1)}, bf16[6,1,4,64,128]{4,3,2,1,0:T(8,128)(2,1)}, f32[6,1,4]{2,1,0:T(1,128)}, f32[6,1,4,64,128]{4,3,2,1,0:T(8,128)S(1)}, /*index=5*/s32[]{:T(128)}, s32[]{:T(128)}) while((s32[]{:T(128)}, f32[1,4,64,128]{3,2,1,0:T(8,128)S(1)}, ...), condition=%wide.region_14.15_spmd.clone, body=%wide.region_13.14_spmd.clone.sunk | while | flops 131075 | bytes 589980 | solution.py:153
  242.8 2.0 fusion.113
  250.7 2.8 fusion.19
  253.6 10.1 %while.60 = (s32[]{:T(128)}, f32[1,4,64,128]{3,2,1,0:T(8,128)S(1)}, bf16[6,1,4,64,128]{4,3,2,1,0:T(8,128)(2,1)S(1)}, f32[6,1,4]{2,1,0:T(1,128)}, f32[6,1,4,64,128]{4,3,2,1,0:T(8,128)}, /*index=5*/s32[]{:T(128)}, s32[]{:T(128)}) while((s32[]{:T(128)}, f32[1,4,64,128]{3,2,1,0:T(8,128)S(1)}, ...), condition=%wide.region_4.5_spmd.clone, body=%wide.region_3.4_spmd.clone.sunk | while | flops 131075 | bytes 589980 | solution.py:153
  263.7 1.4 fusion.32
  266.9 52.0 %all-gather.11.cloned.1.call-done = f32[16,4,64,128]{3,2,1,0:T(8,128)} async-done(((f32[1,4,64,128]{3,2,1,0:T(8,128)}), f32[16,4,64,128]{3,2,1,0:T(8,128)}) %all-gather.11.cloned.1.call-update) | async-done | bytes 2097168 | tf_op jit(solution)/shard_map/all_gather | solution.py:71
  318.9 27.4 %while.63 = (s32[]{:T(128)}, f32[4]{0:T(128)S(1)}, f32[4,64,128]{2,1,0:T(8,128)S(1)}, s32[]{:T(128)}, f32[16,4]{1,0:T(8,128)}, /*index=5*/f32[16,4,64,128]{3,2,1...) while((s32[]{:T(128)}, f32[4]{0:T(128)S(1)}, f32[4,64,128]{2,1,0:T(8,128)S(1)}, ...), condition=%wide.region_18.19_spmd.clone, body=%wide.region_17.18_spmd.clone.sunk | while | flops 131092 | bytes 393481 | solution.py:82
  346.4 2.7 fusion.29
  349.1 4.5 rev.20
  353.6 35.5 %all-gather.9.cloned.1.call-done = f32[16,4,64,128]{3,2,1,0:T(8,128)} async-done(((f32[1,4,64,128]{3,2,1,0:T(8,128)}), f32[16,4,64,128]{3,2,1,0:T(8,128)}) %all-gather.9.cloned.1.call-update) | async-done | bytes 2097168 | tf_op jit(solution)/shard_map/all_gather | solution.py:71
  389.1 27.4 %while.61 = (s32[]{:T(128)}, f32[4]{0:T(128)S(1)}, f32[4,64,128]{2,1,0:T(8,128)S(1)}, s32[]{:T(128)}, f32[16,4]{1,0:T(8,128)}, /*index=5*/f32[16,4,64,128]{3,2,1,0:T(8,128)}, s32[]{:T(128)}, s32[]{:T(128)}) while((s32[]{:T(128)}, f32[4]{0:T(128)S(1)}, f32[4,64,128]{2,1,0:T(8,128)S(1)}, s32[]{:T(128)}, f32[16,4]{1,0:T(8,128)}, ...), condition=%wide.region_8.9_spmd.clone, body=%wide.region_7.8_spmd.clone.sunk | while | flops 131088 | bytes 393419 | solution.py:82
  416.5 2.9 fusion.27
  419.4 5.5 %multiply_reduce_fusion = (f32[768]{0:T(1024)S(1)}, f32[768,256]{0,1:T(8,128)S(1)}) fusion(bf16[768,4096]{1,0:T(8,128)(2,1)} %copy-done.1, bf16[4096,256]{1,0:T(8,128)(2,1)} %param.37, f32[768,4,64]{0,2,1:T(8,128)} %fusion.27), kind=kOutput, calls=%fused_computation.95 | convolution fusion | flops 1612381440 | bytes 9964544 | tf_op jit(solution)/shard_map/dot_general | solution.py:247
  425.9 41.1 %all-gather.13.cloned.1.call-done = bf16[768,2048]{0,1:T(8,128)(2,1)} async-done(((bf16[768,256]{0,1:T(8,128)(2,1)}), bf16[768,2048]{0,1:T(8,128)(2,1)}) %all-gather.13.cloned.1.call-update) | async-done | bytes 3145744 | tf_op jit(solution)/shard_map/all_gather | solution.py:297
  467.0 4.8 add_convert_fusion
  (340 shorter events, 121.0 us)
Async XLA Ops:
  6.5 460.5 %copy-start = (bf16[2048,512]{1,0:T(8,128)(2,1)S(1)}, bf16[2048,512]{1,0:T(8,128)(2,1)}, u32[]{:S(2)}) copy-start(bf16[2048,512]{1,0:T(8,128)(2,1)} %param.49) | copy-start | bytes 6291460
  6.6 27.5 %copy-start.51 = (f32[3,256]{1,0:T(4,128)S(1)}, f32[3,256]{1,0:T(4,128)}, u32[]{:S(2)}) copy-start(f32[3,256]{1,0:T(4,128)} %param.42) | copy-start | bytes 9220
  6.6 27.5 %copy-start.52 = (f32[3,128]{1,0:T(4,128)S(1)}, f32[3,128]{1,0:T(4,128)}, u32[]{:S(2)}) copy-start(f32[3,128]{1,0:T(4,128)} %param.43) | copy-start | bytes 4612
  6.6 27.5 %copy-start.54 = (f32[2,4]{1,0:T(2,128)S(1)}, f32[2,4]{1,0:T(2,128)}, u32[]{:S(2)}) copy-start(f32[2,4]{1,0:T(2,128)} %param.46) | copy-start | bytes 100
  6.6 27.6 %copy-start.53 = (f32[3,128]{1,0:T(4,128)S(1)}, f32[3,128]{1,0:T(4,128)}, u32[]{:S(2)}) copy-start(f32[3,128]{1,0:T(4,128)} %param.44) | copy-start | bytes 4612
  6.6 27.6 %copy-start.24 = (bf16[32,4096]{1,0:T(8,128)(2,1)S(1)}, bf16[32,4096]{1,0:T(8,128)(2,1)}, u32[]{:S(2)}) copy-start(bf16[32,4096]{1,0:T(8,128)(2,1)} %param.30) | copy-start | bytes 786436
  6.6 94.5 %all-gather.7.cloned.1.call-start = ((), (), s32[]{:S(2)}) async-start(), calls=%async_computation.1 | async-start | bytes 9437184 | tf_op jit(solution)/shard_map/all_gather | solution.py:221
  7.4 55.8 %copy-start.31 = (f32[4096]{0:T(1024)S(1)}, f32[4096]{0:T(1024)}, u32[]{:S(2)}) copy-start(f32[4096]{0:T(1024)} %param.36) | copy-start | bytes 49156
  7.4 56.0 %copy-start.28 = (bf16[2,4096,4]{1,2,0:T(4,128)(2,1)S(1)}, bf16[2,4096,4]{1,2,0:T(4,128)(2,1)}, u32[]{:S(2)}) copy-start(bf16[2,4096,4]{1,2,0:T(4,128)(2,1)} %param.41) | copy-start | bytes 196612
  8.9 36.5 %all-to-all-start = ((f32[16,1,2560]{2,1,0:T(1,128)}), f32[16,1,2560]{2,1,0:T(1,128)S(1)}, u32[]{:S(2)}, u32[]{:S(2)}) async-start(f32[16,1,2560]{2,1,0:T(1,128)} %broadcast_in_dim.34), calls=%async_computation | async-start | bytes 327680 | tf_op jit(solution)/shard_map/all_to_all | solution.py:13
  33.4 285.4 %all-gather.11.cloned.1.call-start = ((), (), s32[]{:S(2)}) async-start(), calls=%async_computation.3 | async-start | bytes 2228224 | tf_op jit(solution)/shard_map/all_gather | solution.py:71
  34.4 59.1 %copy-start.41 = (f32[1,512]{1,0:T(1,128)}, f32[1,512]{1,0:T(1,128)S(1)}, u32[]{:S(2)}) copy-start(f32[1,512]{1,0:T(1,128)S(1)} %get-tuple-element.663) | copy-start | bytes 6148
  34.5 59.1 %copy-start.42 = (f32[1,512]{1,0:T(1,128)}, f32[1,512]{1,0:T(1,128)S(1)}, u32[]{:S(2)}) copy-start(f32[1,512]{1,0:T(1,128)S(1)} %get-tuple-element.664) | copy-start | bytes 6148
  34.5 59.1 %copy-start.43 = (f32[1,512]{1,0:T(1,128)}, f32[1,512]{1,0:T(1,128)S(1)}, u32[]{:S(2)}) copy-start(f32[1,512]{1,0:T(1,128)S(1)} %get-tuple-element.665) | copy-start | bytes 6148
  45.5 17.7 %copy-start.37 = (f32[2560]{0:T(1024)}, f32[2560]{0:T(1024)S(1)}, u32[]{:S(2)}) copy-start(f32[2560]{0:T(1024)S(1)} %reduce_sum.36) | copy-start | bytes 30724
  63.9 3.2 copy-start.18
  93.6 2.7 copy-start.48
  101.1 4.6 copy-start.2
  105.7 3.1 copy-start.6
  108.8 8.3 %copy-start.1 = (bf16[768,4096]{1,0:T(8,128)(2,1)}, bf16[768,4096]{1,0:T(8,128)(2,1)S(1)}, u32[]{:S(2)}) copy-start(bf16[768,4096]{1,0:T(8,128)(2,1)S(1)} %fusion.8) | copy-start | bytes 18874372
  111.1 8.0 %copy-start.14 = (bf16[768,128]{0,1:T(8,128)(2,1)}, bf16[768,128]{0,1:T(8,128)(2,1)S(1)}, u32[]{:S(2)}) copy-start(bf16[768,128]{0,1:T(8,128)(2,1)S(1)} %convolution_convert_fusion.2) | copy-start | bytes 589828
  111.1 2.3 copy-start.19
  113.4 5.7 %copy-start.16 = (bf16[768,128]{0,1:T(8,128)(2,1)}, bf16[768,128]{0,1:T(8,128)(2,1)S(1)}, u32[]{:S(2)}) copy-start(bf16[768,128]{0,1:T(8,128)(2,1)S(1)} %convolution_convert_fusion.3) | copy-start | bytes 589828
  115.4 3.7 copy-start.23
  119.1 6.8 %copy-start.40 = (f32[2,4,768]{2,1,0:T(4,128)S(1)}, f32[2,4,768]{2,1,0:T(4,128)}, u32[]{:S(2)}) copy-start(f32[2,4,768]{2,1,0:T(4,128)} %param.47) | copy-start | bytes 73732
  119.9 84.0 %collective-permute-start.1 = (bf16[1,512]{0,1:T(8,128)(2,1)}, bf16[1,512]{0,1:T(8,128)(2,1)S(1)}, u32[]{:S(2)}, u32[]{:S(2)}) collective-permute-start(bf16[1,512]{0,1:T(8,128)(2,1)} %get-tuple-element.645), channel_id=1, source_target_pairs={{8,0},{16,8},{24,16},{32,24},{40,32},{48,40},{56,48},{64,56},{72,6... | collective-permute-start | bytes 3080 | tf_op jit(solution)/shard_map/ppermute | solution.py:62
  121.2 82.7 %collective-permute-start = (bf16[1,512]{0,1:T(8,128)(2,1)}, bf16[1,512]{0,1:T(8,128)(2,1)}, u32[]{:S(2)}, u32[]{:S(2)}) collective-permute-start(bf16[1,512]{0,1:T(8,128)(2,1)} %get-tuple-element.644), channel_id=1, source_target_pairs={{0,8},{8,16},{16,24},{24,32},{32,40},{40,48},{48,56},{56,64},{64,7... | collective-permute-start | bytes 3080 | tf_op jit(solution)/shard_map/ppermute | solution.py:60
  150.0 53.9 %copy-start.15 = (bf16[768,128]{0,1:T(8,128)(2,1)S(1)}, bf16[768,128]{0,1:T(8,128)(2,1)}, u32[]{:S(2)}) copy-start(bf16[768,128]{0,1:T(8,128)(2,1)} %copy-done.14) | copy-start | bytes 589828
  150.0 53.9 %copy-start.17 = (bf16[768,128]{0,1:T(8,128)(2,1)S(1)}, bf16[768,128]{0,1:T(8,128)(2,1)}, u32[]{:S(2)}) copy-start(bf16[768,128]{0,1:T(8,128)(2,1)} %copy-done.16) | copy-start | bytes 589828
  224.2 3.5 copy-start.34
  227.8 2.3 copy-start.29
  240.7 4.1 copy-start.10
  240.8 4.1 copy-start.44
  240.8 4.1 copy-start.47
  241.5 147.6 %all-gather.9.cloned.1.call-start = ((), (), s32[]{:S(2)}) async-start(), calls=%async_computation.2 | async-start | bytes 2228224 | tf_op jit(solution)/shard_map/all_gather | solution.py:71
  253.6 10.1 %copy-start.11 = (bf16[768,128]{1,0:T(8,128)(2,1)S(1)}, bf16[768,128]{1,0:T(8,128)(2,1)}, u32[]{:S(2)}) copy-start(bf16[768,128]{1,0:T(8,128)(2,1)} %copy.303) | copy-start | bytes 589828
  253.6 10.1 %copy-start.32 = (f32[6,128,4]{1,2,0:T(4,128)S(1)}, f32[6,128,4]{1,2,0:T(4,128)}, u32[]{:S(2)}) copy-start(f32[6,128,4]{1,2,0:T(4,128)} %copy.306) | copy-start | bytes 36868
  265.2 53.7 %copy-start.46 = (f32[4]{0:T(128)S(1)}, f32[4]{0:T(128)}, u32[]{:S(2)}) copy-start(f32[4]{0:T(128)} %custom-call.4) | copy-start | bytes 52
  266.8 79.6 %copy-start.5 = (f32[512,256]{0,1:T(8,128)S(1)}, f32[512,256]{0,1:T(8,128)}, u32[]{:S(2)}) copy-start(f32[512,256]{0,1:T(8,128)} %copy.318) | copy-start | bytes 1572868
  266.8 79.6 %copy-start.36 = (f32[768,4]{0,1:T(4,128)S(1)}, f32[768,4]{0,1:T(4,128)}, u32[]{:S(2)}) copy-start(f32[768,4]{0,1:T(4,128)} %get-tuple-element.636) | copy-start | bytes 36868
  266.8 79.6 %copy-start.39 = (f32[512,4]{0,1:T(4,128)S(1)}, f32[512,4]{0,1:T(4,128)}, u32[]{:S(2)}) copy-start(f32[512,4]{0,1:T(4,128)} %fusion.94) | copy-start | bytes 24580
  266.8 200.2 %all-gather.13.cloned.1.call-start = ((), (), s32[]{:S(2)}) async-start(), calls=%async_computation.4 | async-start | bytes 3538944 | tf_op jit(solution)/shard_map/all_gather | solution.py:297
  346.4 42.7 %copy-start.45 = (f32[4]{0:T(128)S(1)}, f32[4]{0:T(128)}, u32[]{:S(2)}) copy-start(f32[4]{0:T(128)} %custom-call.1) | copy-start | bytes 52
  349.1 67.4 %copy-start.12 = (bf16[768,128]{1,0:T(8,128)(2,1)S(1)}, bf16[768,128]{1,0:T(8,128)(2,1)}, u32[]{:S(2)}) copy-start(bf16[768,128]{1,0:T(8,128)(2,1)} %copy.303) | copy-start | bytes 589828
  349.1 67.4 %copy-start.35 = (f32[768,4]{0,1:T(4,128)S(1)}, f32[768,4]{0,1:T(4,128)}, u32[]{:S(2)}) copy-start(f32[768,4]{0,1:T(4,128)} %get-tuple-element.632) | copy-start | bytes 36868
  349.1 67.4 %copy-start.38 = (f32[512,4]{0,1:T(4,128)S(1)}, f32[512,4]{0,1:T(4,128)}, u32[]{:S(2)}) copy-start(f32[512,4]{0,1:T(4,128)} %fusion.95) | copy-start | bytes 24580
  419.4 5.6 %copy-start.55 = (f32[256]{0:T(256)S(1)}, f32[256]{0:T(256)}, u32[]{:S(2)}) copy-start(f32[256]{0:T(256)} %param.48) | copy-start | bytes 3076
  424.9 42.1 %slice-start = ((f32[2560]{0:T(1024)}), f32[512]{0:T(512)S(1)}, s32[]{:S(2)}) async-start(f32[2560]{0:T(1024)} %copy-done.37), calls=%async_computation.5 | async-start | bytes 4096 | tf_op jit(solution)/shard_map/slice | solution.py:26
  (16 other events, 19.5 us)
Sparse Core Ops, SparseCore 0:
  9.3 41.3 all-gather.6
  241.6 77.2 all-gather.10
  320.7 68.3 all-gather.8
  426.0 40.9 all-gather.12
where the time goes:
time: 482 us; the launch traced here: 478 us
  waiting for transfers between devices  140 us (29%)
  other arithmetic  98.2 us (20%)
  blocking collectives  85.9 us (18%)
  local copies, waits for them, and re-layouts  67.5 us (14%)
  matrix products  40.4 us (8%)
  starting transfers between devices  30.8 us (6%)
  between operations  14.2 us (3%)
    all_gather x2, waiting for transfers between devices, entering(): everything = jax.tree.map(lambda part: lax.all_gather(part, axis), x)  87.5 us
    all_gather x2, blocking collectives, entering(): everything = jax.tree.map(lambda part: lax.all_gather(part, axis), x)  42.4 us
    all_gather x1, waiting for transfers between devices, on_device(): lax.all_gather(normed, ('tp', 'dp'), axis=1, tiled=True)  41.1 us
    select_n x32, other arithmetic, turn(): return jax.tree.map(lambda a, b: jnp.where(reached, a, b), new, before)  31.6 us
    all_gather x1, blocking collectives, rows_first(): out = lax.all_gather(both, axis, axis=0, tiled=True)  25.9 us
    all_to_all x1, starting transfers between devices, copy_for_each(): return lax.all_to_all(copies, axis, split_axis=0, concat_axis=0, tiled=True)  24.5 us
    exp x32, other arithmetic, chain_step(): jnp.exp(later[0])[:, None, None] * preceding_entries[1] + later[1]  22.3 us
    all_gather x1, blocking collectives, side_by_side(): lax.all_gather(both, axis, axis=dim, tiled=True)  17.6 us
  transfers between devices with their start and end apart: 7, of which 4 were waited for; matrix products, arithmetic and copies ran while one was open for 22% of the time, Pallas kernels for 0%

commit v1 on v0

--- a/solution.py
+++ b/solution.py
@@ -293,11 +293,16 @@
     both = (forward_out + jnp.flip(backward_out, 0)).reshape(length, -1)
     gated = both * jax.nn.silu(gate_in.astype(jnp.float32))
     normed = group_norm(gated, group_count, group_gain)
-    mix = jnp.dot(
-        lax.all_gather(normed, ("tp", "dp"), axis=1, tiled=True),
-        output_weight,
-        preferred_element_type=jnp.float32,
-    )
+    run_table = lambda array_here: jnp.concatenate(
+        lax.all_to_all(
+            jnp.stack([array_here for _ in range(lax.axis_size(("tp", "dp")))], 0),
+            ("tp", "dp"),
+            0,
+            0,
+        ),
+        1,
+    )
+    mix = jnp.dot(run_table(normed), output_weight, preferred_element_type=jnp.float32)
     out_start = lax.axis_index(("tp", "dp")) * output_weight.shape[1]
     residual = lax.dynamic_slice_in_dim(full_rows, out_start, output_weight.shape[1], 1).astype(
         jnp.float32

time: 482 us -> 494 us (1.025)
  starting transfers between devices: 30.8 us -> 45.5 us
    all_gather x1 -> x0, waiting for transfers between devices: 41.1 us -> none  [on_device(): lax.all_gather(normed, ('tp', 'dp'), axis=1, tiled=True)]
    all_to_all x0 -> x1, waiting for transfers between devices: none -> 37.6 us  [on_device(): lax.all_to_all(jnp.stack([array_here for _ in range(lax.axis_size(('tp',...]
    all_to_all x0 -> x1, starting transfers between devices: none -> 14.8 us  [on_device(): lax.all_to_all(jnp.stack([array_here for _ in range(lax.axis_size(('tp',...]
    another operation x12 -> x13, local copies, waits for them, and re-layouts: 13.4 us -> 15.3 us
where the time goes in v1:
time: 494 us; the launch traced here: 490 us
  waiting for transfers between devices  136 us (28%)
  other arithmetic  97.2 us (20%)
  blocking collectives  86.1 us (17%)
  local copies, waits for them, and re-layouts  69.4 us (14%)
  starting transfers between devices  45.5 us (9%)
  matrix products  40.4 us (8%)
  between operations  14.1 us (3%)
    all_gather x2, waiting for transfers between devices, entering(): everything = jax.tree.map(lambda part: lax.all_gather(part, axis), x)  87 us
    all_gather x2, blocking collectives, entering(): everything = jax.tree.map(lambda part: lax.all_gather(part, axis), x)  42.6 us
    all_to_all x1, waiting for transfers between devices, on_device(): lax.all_to_all(jnp.stack([array_here for _ in range(lax.axis_size(('tp',...  37.6 us
    select_n x32, other arithmetic, turn(): return jax.tree.map(lambda a, b: jnp.where(reached, a, b), new, before)  31.6 us
    all_gather x1, blocking collectives, rows_first(): out = lax.all_gather(both, axis, axis=0, tiled=True)  25.9 us
    all_to_all x1, starting transfers between devices, copy_for_each(): return lax.all_to_all(copies, axis, split_axis=0, concat_axis=0, tiled=True)  24.5 us
    exp x32, other arithmetic, chain_step(): jnp.exp(later[0])[:, None, None] * preceding_entries[1] + later[1]  22.2 us
    all_gather x1, blocking collectives, side_by_side(): lax.all_gather(both, axis, axis=dim, tiled=True)  17.6 us
  transfers between devices with their start and end apart: 7, of which 4 were waited for; matrix products, arithmetic and copies ran while one was open for 22% of the time, Pallas kernels for 0%

profile of v1, /device:TPU:33, one launch (start us, length us, event | category | flops | bytes accessed | tf_op | source)
XLA Modules:
  0.0 490.4 jit_solution(4143906756519044354)
XLA Ops:
  8.9 24.5 %all-to-all-start = ((f32[16,1,2560]{2,1,0:T(1,128)}), f32[16,1,2560]{2,1,0:T(1,128)S(1)}, u32[]{:S(2)}, u32[]{:S(2)}) async-start(f32[16,1,2560]{2,1,0:T(1,128)} %broadcast_in_dim.34), calls=%async_computation | async-start | bytes 327680 | tf_op jit(solution)/shard_map/all_to_all | solution.py:13
  34.5 10.9 %all-to-all-done = f32[16,1,2560]{2,1,0:T(1,128)S(1)} async-done(((f32[16,1,2560]{2,1,0:T(1,128)}), f32[16,1,2560]{2,1,0:T(1,128)S(1)}, u32[]{:S(2)}, u32[]{:S(2)}) %all-to-all-start) | async-done | bytes 163872 | tf_op jit(solution)/shard_map/all_to_all | solution.py:13
  45.6 17.6 %all_gather.22 = f32[4,4096]{1,0:T(4,128)S(1)} all-gather(f32[4,512]{1,0:T(4,128)S(1)} %pad_maximum_fusion.9), channel_id=1, replica_groups=mesh['grp'=2,'sp'=16,'tp'=4,'dp'=2] {'tp','dp'}, dimensions={1}, use_global_device_ids=true | all-gather | bytes 73728 | tf_op jit(solution)/shard_map/all_gather | solution.py:35
  63.9 1.7 convolution_convert_fusion.5
  67.6 25.9 %all_gather.25 = bf16[512,520]{1,0:T(8,128)(2,1)S(1)} all-gather(bf16[32,520]{1,0:T(8,128)(2,1)S(1)} %pad_maximum_fusion.7), channel_id=1, replica_groups=mesh['grp'=2,'sp'=16,'tp'=4,'dp'=2] {'sp'}, dimensions={0}, use_global_device_ids=true | all-gather | bytes 565760 | tf_op jit(solution)/shard_map/all_gather | solution.py:42
  96.3 2.4 reduce-window.24
  101.1 4.2 fusion.4
  105.7 3.1 fusion.8
  108.8 2.2 convolution_convert_fusion.2
  111.1 2.2 convolution_convert_fusion.3
  113.4 2.0 convolution_convert_fusion.1
  115.4 1.7 fusion.38
  117.1 2.0 fusion.37
  121.2 4.7 collective-permute-start
  128.4 3.3 rev.19
  136.1 1.7 copy.342
  141.7 2.2 reduce-window.20
  148.1 1.7 fusion.107
  149.8 1.7 fusion.106
  151.5 1.8 copy.330
  153.3 1.7 copy.327
  159.6 1.7 copy.307
  161.4 20.4 %all-gather.1 = f32[16,1,4]{2,1,0:T(1,128)} all-gather(f32[1,1,4]{2,1,0:T(1,128)} %bitcast.354), channel_id=1, replica_groups=mesh['grp'=2,'sp'=16,'tp'=4,'dp'=2] {'sp'}, dimensions={0}, use_global_device_ids=true | all-gather | bytes 272 | tf_op jit(solution)/shard_map/all_gather | solution.py:71
  181.8 22.1 %all-gather = f32[16,1,4]{2,1,0:T(1,128)} all-gather(f32[1,1,4]{2,1,0:T(1,128)} %bitcast.355), channel_id=1, replica_groups=mesh['grp'=2,'sp'=16,'tp'=4,'dp'=2] {'sp'}, dimensions={0}, use_global_device_ids=true | all-gather | bytes 272 | tf_op jit(solution)/shard_map/all_gather | solution.py:71
  204.0 4.9 %divide_multiply_fusion = f32[768,512]{0,1:T(8,128)S(1)} fusion(bf16[1,512]{0,1:T(8,128)(2,1)S(1)} %collective-permute-done.1, bf16[768,128]{0,1:T(8,128)(2,1)S(1)} %copy-done.15, bf16[768,128]{0,1:T(8,128)(2,1)S(1)} %copy-done.17, bf16[768,256]{0,1:T(8,128)(2,1)} %copy-done.23, bf16[1,512]{0,1:T(8,128)(2,1)} %collective-permute-done, f32[512]{0:T(512)} %bitcast.342, ...), kind=kLoop, calls=%fused_computation.35 | loop fusion | flops 12189696 | bytes 2367488 | tf_op jit(solution)/shard_map/jit(silu)/mul | solution.py:97
  209.8 3.8 reverse.6
  213.6 1.8 copy.304
  215.3 3.8 reverse.7
  219.1 1.7 copy.305
  220.8 1.8 copy.324
  222.6 1.7 copy.325
  225.4 2.4 rev.18
  232.6 8.3 %while.62 = (s32[]{:T(128)}, f32[1,4,64,128]{3,2,1,0:T(8,128)S(1)}, bf16[6,1,4,64,128]{4,3,2,1,0:T(8,128)(2,1)}, f32[6,1,4]{2,1,0:T(1,128)}, f32[6,1,4,64,128]{4,3,2,1,0:T(8,128)S(1)}, /*index=5*/s32[]{:T(128)}, s32[]{:T(128)}) while((s32[]{:T(128)}, f32[1,4,64,128]{3,2,1,0:T(8,128)S(1)}, ...), condition=%wide.region_14.15_spmd.clone, body=%wide.region_13.14_spmd.clone.sunk | while | flops 131075 | bytes 589980 | solution.py:153
  243.0 2.1 fusion.113
  250.9 2.8 fusion.19
  253.8 10.3 %while.60 = (s32[]{:T(128)}, f32[1,4,64,128]{3,2,1,0:T(8,128)S(1)}, bf16[6,1,4,64,128]{4,3,2,1,0:T(8,128)(2,1)S(1)}, f32[6,1,4]{2,1,0:T(1,128)}, f32[6,1,4,64,128]{4,3,2,1,0:T(8,128)}, /*index=5*/s32[]{:T(128)}, s32[]{:T(128)}) while((s32[]{:T(128)}, f32[1,4,64,128]{3,2,1,0:T(8,128)S(1)}, ...), condition=%wide.region_4.5_spmd.clone, body=%wide.region_3.4_spmd.clone.sunk | while | flops 131075 | bytes 589980 | solution.py:153
  267.2 51.8 %all-gather.10.cloned.1.call-done = f32[16,4,64,128]{3,2,1,0:T(8,128)} async-done(((f32[1,4,64,128]{3,2,1,0:T(8,128)}), f32[16,4,64,128]{3,2,1,0:T(8,128)}) %all-gather.10.cloned.1.call-update) | async-done | bytes 2097168 | tf_op jit(solution)/shard_map/all_gather | solution.py:71
  319.0 27.4 %while.63 = (s32[]{:T(128)}, f32[4]{0:T(128)S(1)}, f32[4,64,128]{2,1,0:T(8,128)S(1)}, s32[]{:T(128)}, f32[16,4]{1,0:T(8,128)}, /*index=5*/f32[16,4,64,128]{3,2,1...) while((s32[]{:T(128)}, f32[4]{0:T(128)S(1)}, f32[4,64,128]{2,1,0:T(8,128)S(1)}, ...), condition=%wide.region_18.19_spmd.clone, body=%wide.region_17.18_spmd.clone.sunk | while | flops 131092 | bytes 393481 | solution.py:82
  346.5 2.7 fusion.29
  349.2 4.5 rev.20
  353.7 35.2 %all-gather.8.cloned.1.call-done = f32[16,4,64,128]{3,2,1,0:T(8,128)} async-done(((f32[1,4,64,128]{3,2,1,0:T(8,128)}), f32[16,4,64,128]{3,2,1,0:T(8,128)}) %all-gather.8.cloned.1.call-update) | async-done | bytes 2097168 | tf_op jit(solution)/shard_map/all_gather | solution.py:71
  388.9 27.3 %while.61 = (s32[]{:T(128)}, f32[4]{0:T(128)S(1)}, f32[4,64,128]{2,1,0:T(8,128)S(1)}, s32[]{:T(128)}, f32[16,4]{1,0:T(8,128)}, /*index=5*/f32[16,4,64,128]{3,2,1,0:T(8,128)}, s32[]{:T(128)}, s32[]{:T(128)}) while((s32[]{:T(128)}, f32[4]{0:T(128)S(1)}, f32[4,64,128]{2,1,0:T(8,128)S(1)}, s32[]{:T(128)}, f32[16,4]{1,0:T(8,128)}, ...), condition=%wide.region_8.9_spmd.clone, body=%wide.region_7.8_spmd.clone.sunk | while | flops 131088 | bytes 393419 | solution.py:82
  416.2 2.8 fusion.27
  419.1 5.5 %multiply_reduce_fusion = (f32[768]{0:T(1024)S(1)}, f32[768,256]{0,1:T(8,128)S(1)}) fusion(bf16[768,4096]{1,0:T(8,128)(2,1)} %copy-done.1, bf16[4096,256]{1,0:T(8,128)(2,1)} %param.37, f32[768,4,64]{0,2,1:T(8,128)} %fusion.27), kind=kOutput, calls=%fused_computation.95 | convolution fusion | flops 1612381440 | bytes 9964544 | tf_op jit(solution)/shard_map/dot_general | solution.py:247
  424.7 1.9 stack.53
  426.6 14.8 %all-to-all-start.1 = ((bf16[8,768,256]{1,2,0:T(8,128)(2,1)}), bf16[8,768,256]{1,2,0:T(8,128)(2,1)}, u32[]{:S(2)}, u32[]{:S(2)}) async-start(bf16[8,768,256]{1,2,0:T(8,128)(2,1)} %stack.53), calls=%async_computation.1 | async-start | bytes 6291456 | tf_op jit(solution)/shard_map/all_to_all | solution.py:297
  441.4 37.6 %all-to-all-done.1 = bf16[8,768,256]{1,2,0:T(8,128)(2,1)} async-done(((bf16[8,768,256]{1,2,0:T(8,128)(2,1)}), bf16[8,768,256]{1,2,0:T(8,128)(2,1)}, u32[]{:S(2)}, u32[]{:S(2)}) %all-to-all-start.1) | async-done | bytes 3145760 | tf_op jit(solution)/shard_map/all_to_all | solution.py:297
  479.1 4.8 add_convert_fusion
  (340 shorter events, 122.8 us)
Async XLA Ops:
  6.5 472.5 %copy-start = (bf16[2048,512]{1,0:T(8,128)(2,1)S(1)}, bf16[2048,512]{1,0:T(8,128)(2,1)}, u32[]{:S(2)}) copy-start(bf16[2048,512]{1,0:T(8,128)(2,1)} %param.49) | copy-start | bytes 6291460
  6.6 27.6 %copy-start.51 = (f32[3,256]{1,0:T(4,128)S(1)}, f32[3,256]{1,0:T(4,128)}, u32[]{:S(2)}) copy-start(f32[3,256]{1,0:T(4,128)} %param.42) | copy-start | bytes 9220
  6.6 27.5 %copy-start.52 = (f32[3,128]{1,0:T(4,128)S(1)}, f32[3,128]{1,0:T(4,128)}, u32[]{:S(2)}) copy-start(f32[3,128]{1,0:T(4,128)} %param.43) | copy-start | bytes 4612
  6.6 27.5 %copy-start.54 = (f32[2,4]{1,0:T(2,128)S(1)}, f32[2,4]{1,0:T(2,128)}, u32[]{:S(2)}) copy-start(f32[2,4]{1,0:T(2,128)} %param.46) | copy-start | bytes 100
  6.6 27.6 %copy-start.53 = (f32[3,128]{1,0:T(4,128)S(1)}, f32[3,128]{1,0:T(4,128)}, u32[]{:S(2)}) copy-start(f32[3,128]{1,0:T(4,128)} %param.44) | copy-start | bytes 4612
  6.6 27.6 %copy-start.24 = (bf16[32,4096]{1,0:T(8,128)(2,1)S(1)}, bf16[32,4096]{1,0:T(8,128)(2,1)}, u32[]{:S(2)}) copy-start(bf16[32,4096]{1,0:T(8,128)(2,1)} %param.30) | copy-start | bytes 786436
  6.6 94.5 %all-gather.6.cloned.1.call-start = ((), (), s32[]{:S(2)}) async-start(), calls=%async_computation.2 | async-start | bytes 9437184 | tf_op jit(solution)/shard_map/all_gather | solution.py:221
  7.4 55.8 %copy-start.31 = (f32[4096]{0:T(1024)S(1)}, f32[4096]{0:T(1024)}, u32[]{:S(2)}) copy-start(f32[4096]{0:T(1024)} %param.36) | copy-start | bytes 49156
  7.4 56.0 %copy-start.28 = (bf16[2,4096,4]{1,2,0:T(4,128)(2,1)S(1)}, bf16[2,4096,4]{1,2,0:T(4,128)(2,1)}, u32[]{:S(2)}) copy-start(bf16[2,4096,4]{1,2,0:T(4,128)(2,1)} %param.41) | copy-start | bytes 196612
  8.9 36.5 %all-to-all-start = ((f32[16,1,2560]{2,1,0:T(1,128)}), f32[16,1,2560]{2,1,0:T(1,128)S(1)}, u32[]{:S(2)}, u32[]{:S(2)}) async-start(f32[16,1,2560]{2,1,0:T(1,128)} %broadcast_in_dim.34), calls=%async_computation | async-start | bytes 327680 | tf_op jit(solution)/shard_map/all_to_all | solution.py:13
  33.4 285.6 %all-gather.10.cloned.1.call-start = ((), (), s32[]{:S(2)}) async-start(), calls=%async_computation.4 | async-start | bytes 2228224 | tf_op jit(solution)/shard_map/all_gather | solution.py:71
  34.4 59.1 %copy-start.41 = (f32[1,512]{1,0:T(1,128)}, f32[1,512]{1,0:T(1,128)S(1)}, u32[]{:S(2)}) copy-start(f32[1,512]{1,0:T(1,128)S(1)} %get-tuple-element.663) | copy-start | bytes 6148
  34.5 59.1 %copy-start.42 = (f32[1,512]{1,0:T(1,128)}, f32[1,512]{1,0:T(1,128)S(1)}, u32[]{:S(2)}) copy-start(f32[1,512]{1,0:T(1,128)S(1)} %get-tuple-element.664) | copy-start | bytes 6148
  34.5 59.1 %copy-start.43 = (f32[1,512]{1,0:T(1,128)}, f32[1,512]{1,0:T(1,128)S(1)}, u32[]{:S(2)}) copy-start(f32[1,512]{1,0:T(1,128)S(1)} %get-tuple-element.665) | copy-start | bytes 6148
  45.5 17.7 %copy-start.37 = (f32[2560]{0:T(1024)}, f32[2560]{0:T(1024)S(1)}, u32[]{:S(2)}) copy-start(f32[2560]{0:T(1024)S(1)} %reduce_sum.36) | copy-start | bytes 30724
  63.9 3.2 copy-start.18
  93.6 2.6 copy-start.48
  101.1 4.6 copy-start.2
  105.7 3.1 copy-start.6
  108.8 8.3 %copy-start.1 = (bf16[768,4096]{1,0:T(8,128)(2,1)}, bf16[768,4096]{1,0:T(8,128)(2,1)S(1)}, u32[]{:S(2)}) copy-start(bf16[768,4096]{1,0:T(8,128)(2,1)S(1)} %fusion.8) | copy-start | bytes 18874372
  111.1 8.0 %copy-start.14 = (bf16[768,128]{0,1:T(8,128)(2,1)}, bf16[768,128]{0,1:T(8,128)(2,1)S(1)}, u32[]{:S(2)}) copy-start(bf16[768,128]{0,1:T(8,128)(2,1)S(1)} %convolution_convert_fusion.2) | copy-start | bytes 589828
  111.1 2.3 copy-start.19
  113.3 5.7 %copy-start.16 = (bf16[768,128]{0,1:T(8,128)(2,1)}, bf16[768,128]{0,1:T(8,128)(2,1)S(1)}, u32[]{:S(2)}) copy-start(bf16[768,128]{0,1:T(8,128)(2,1)S(1)} %convolution_convert_fusion.3) | copy-start | bytes 589828
  115.4 3.7 copy-start.23
  119.1 6.8 %copy-start.40 = (f32[2,4,768]{2,1,0:T(4,128)S(1)}, f32[2,4,768]{2,1,0:T(4,128)}, u32[]{:S(2)}) copy-start(f32[2,4,768]{2,1,0:T(4,128)} %param.47) | copy-start | bytes 73732
  119.9 84.0 %collective-permute-start.1 = (bf16[1,512]{0,1:T(8,128)(2,1)}, bf16[1,512]{0,1:T(8,128)(2,1)S(1)}, u32[]{:S(2)}, u32[]{:S(2)}) collective-permute-start(bf16[1,512]{0,1:T(8,128)(2,1)} %get-tuple-element.645), channel_id=1, source_target_pairs={{8,0},{16,8},{24,16},{32,24},{40,32},{48,40},{56,48},{64,56},{72,6... | collective-permute-start | bytes 3080 | tf_op jit(solution)/shard_map/ppermute | solution.py:62
  121.2 82.7 %collective-permute-start = (bf16[1,512]{0,1:T(8,128)(2,1)}, bf16[1,512]{0,1:T(8,128)(2,1)}, u32[]{:S(2)}, u32[]{:S(2)}) collective-permute-start(bf16[1,512]{0,1:T(8,128)(2,1)} %get-tuple-element.644), channel_id=1, source_target_pairs={{0,8},{8,16},{16,24},{24,32},{32,40},{40,48},{48,56},{56,64},{64,7... | collective-permute-start | bytes 3080 | tf_op jit(solution)/shard_map/ppermute | solution.py:60
  149.8 54.2 %copy-start.15 = (bf16[768,128]{0,1:T(8,128)(2,1)S(1)}, bf16[768,128]{0,1:T(8,128)(2,1)}, u32[]{:S(2)}) copy-start(bf16[768,128]{0,1:T(8,128)(2,1)} %copy-done.14) | copy-start | bytes 589828
  149.8 54.2 %copy-start.17 = (bf16[768,128]{0,1:T(8,128)(2,1)S(1)}, bf16[768,128]{0,1:T(8,128)(2,1)}, u32[]{:S(2)}) copy-start(bf16[768,128]{0,1:T(8,128)(2,1)} %copy-done.16) | copy-start | bytes 589828
  224.3 3.5 copy-start.34
  227.8 2.3 copy-start.29
  240.9 4.1 copy-start.10
  241.0 4.1 copy-start.44
  241.0 4.1 copy-start.47
  241.7 147.2 %all-gather.8.cloned.1.call-start = ((), (), s32[]{:S(2)}) async-start(), calls=%async_computation.3 | async-start | bytes 2228224 | tf_op jit(solution)/shard_map/all_gather | solution.py:71
  253.8 10.3 %copy-start.11 = (bf16[768,128]{1,0:T(8,128)(2,1)S(1)}, bf16[768,128]{1,0:T(8,128)(2,1)}, u32[]{:S(2)}) copy-start(bf16[768,128]{1,0:T(8,128)(2,1)} %copy.304) | copy-start | bytes 589828
  253.8 10.3 %copy-start.32 = (f32[6,128,4]{1,2,0:T(4,128)S(1)}, f32[6,128,4]{1,2,0:T(4,128)}, u32[]{:S(2)}) copy-start(f32[6,128,4]{1,2,0:T(4,128)} %copy.307) | copy-start | bytes 36868
  265.5 53.5 %copy-start.46 = (f32[4]{0:T(128)S(1)}, f32[4]{0:T(128)}, u32[]{:S(2)}) copy-start(f32[4]{0:T(128)} %custom-call.4) | copy-start | bytes 52
  267.1 79.3 %copy-start.5 = (f32[512,256]{0,1:T(8,128)S(1)}, f32[512,256]{0,1:T(8,128)}, u32[]{:S(2)}) copy-start(f32[512,256]{0,1:T(8,128)} %copy.319) | copy-start | bytes 1572868
  267.1 79.3 %copy-start.36 = (f32[768,4]{0,1:T(4,128)S(1)}, f32[768,4]{0,1:T(4,128)}, u32[]{:S(2)}) copy-start(f32[768,4]{0,1:T(4,128)} %get-tuple-element.636) | copy-start | bytes 36868
  267.1 79.3 %copy-start.39 = (f32[512,4]{0,1:T(4,128)S(1)}, f32[512,4]{0,1:T(4,128)}, u32[]{:S(2)}) copy-start(f32[512,4]{0,1:T(4,128)} %fusion.94) | copy-start | bytes 24580
  346.5 42.4 %copy-start.45 = (f32[4]{0:T(128)S(1)}, f32[4]{0:T(128)}, u32[]{:S(2)}) copy-start(f32[4]{0:T(128)} %custom-call.1) | copy-start | bytes 52
  349.2 67.0 %copy-start.12 = (bf16[768,128]{1,0:T(8,128)(2,1)S(1)}, bf16[768,128]{1,0:T(8,128)(2,1)}, u32[]{:S(2)}) copy-start(bf16[768,128]{1,0:T(8,128)(2,1)} %copy.304) | copy-start | bytes 589828
  349.2 67.0 %copy-start.35 = (f32[768,4]{0,1:T(4,128)S(1)}, f32[768,4]{0,1:T(4,128)}, u32[]{:S(2)}) copy-start(f32[768,4]{0,1:T(4,128)} %get-tuple-element.632) | copy-start | bytes 36868
  349.2 67.0 %copy-start.38 = (f32[512,4]{0,1:T(4,128)S(1)}, f32[512,4]{0,1:T(4,128)}, u32[]{:S(2)}) copy-start(f32[512,4]{0,1:T(4,128)} %fusion.95) | copy-start | bytes 24580
  419.1 5.5 %copy-start.55 = (f32[256]{0:T(256)S(1)}, f32[256]{0:T(256)}, u32[]{:S(2)}) copy-start(f32[256]{0:T(256)} %param.48) | copy-start | bytes 3076
  426.6 52.5 %slice-start = ((f32[2560]{0:T(1024)}), f32[512]{0:T(512)S(1)}, s32[]{:S(2)}) async-start(f32[2560]{0:T(1024)} %copy-done.37), calls=%async_computation.5 | async-start | bytes 4096 | tf_op jit(solution)/shard_map/slice | solution.py:26
  426.6 52.4 %all-to-all-start.1 = ((bf16[8,768,256]{1,2,0:T(8,128)(2,1)}), bf16[8,768,256]{1,2,0:T(8,128)(2,1)}, u32[]{:S(2)}, u32[]{:S(2)}) async-start(bf16[8,768,256]{1,2,0:T(8,128)(2,1)} %stack.53), calls=%async_computation.1 | async-start | bytes 6291456 | tf_op jit(solution)/shard_map/all_to_all | solution.py:297
  (16 other events, 19.4 us)
Sparse Core Ops, SparseCore 0:
  9.3 41.3 all-gather.5
  241.8 77.1 all-gather.9
  320.8 68.0 all-gather.7
